TPU v7x, 32 devices: a whole 2x2x4 slice. The times are simulated.
32 devices in a mesh: sp: 16 (over z, y, x), tp: 2 (over core).
Axes of the slice: x: 2, y: 2, z: 4, core: 2. Of those that a mesh axis runs over, the one named last changes fastest.
Arguments:
- tokens: bfloat16 [8192, 3072], P('sp'), may hold values from -72 to 72
- w_query: bfloat16 [3072, 1024], P('sp', 'tp'), may hold values from -0.109375 to 0.109375
- w_key: bfloat16 [3072, 1024], P('sp', 'tp'), may hold values from -0.109375 to 0.109375
- w_value: bfloat16 [3072, 1024], P('sp', 'tp'), may hold values from -0.4375 to 0.4375
- w_out: bfloat16 [1024, 3072], P('tp', 'sp'), may hold values from -0.1875 to 0.1875
Outputs:
- mixed: bfloat16 [8192, 3072], P(('sp', 'tp'))
- row_lse: float32 [16, 8192], P('tp', 'sp')
All inputs are finite; a program needn't handle non-finite values.
Results may differ from a plain program's by a relative error of at most 0.014.
Values may be sent and summed in bfloat16 or wider, within the bound.
No kernel may reach another device: no remote copies, remote signals or barrier semaphores. Data moves between devices by JAX's collectives and lax.ppermute only.
A program may use at most 64 MiB of HBM per device.

v0:
```python
from functools import partial

import jax
import jax.numpy as jnp
from jax import lax
from jax.experimental import pallas as pl
from jax.experimental.pallas import tpu as pltpu
from jax.sharding import PartitionSpec as P

HEAD_SIZE = 64
KEYS_BEHIND = 128
RATE = 16
CHUNK = RATE * RATE
NEG = -1e30


VMEM = pl.BlockSpec(memory_space=pltpu.VMEM)
SMEM = pl.BlockSpec(memory_space=pltpu.SMEM)


def natural(parts, at):
    parts = list(parts)
    bit = 1
    while bit < len(parts):
        flip = (at & bit) != 0
        parts = [jnp.where(flip, parts[j ^ bit], parts[j]) for j in range(len(parts))]
        bit *= 2
    return parts


def prep_kernel(where_ref, q_ref, k_ref, v_ref, *outs):
    group = len(outs)
    cols = q_ref.shape[1] // group
    for t, ref in enumerate((k_ref, v_ref, q_ref)):
        w = ref[...]
        parts = natural([w[:, b * cols:(b + 1) * cols] for b in range(group)], where_ref[0])
        for j in range(group):
            outs[j][:, t * cols:(t + 1) * cols] = parts[j]


def prep(at, w_query, w_key, w_value, group):
    fan, width = w_query.shape
    return pl.pallas_call(
        prep_kernel,
        in_specs=[SMEM, VMEM, VMEM, VMEM],
        out_specs=[VMEM] * group,
        out_shape=[jax.ShapeDtypeStruct((fan, 3 * width // group), jnp.bfloat16)] * group,
        name="prep",
    )(at, w_query, w_key, w_value)


def collect_kernel(where_ref, *refs):
    pieces, (kv_ref, q_ref) = refs[:-2], refs[-2:]
    fan, two = pieces[0].shape[0], kv_ref.shape[1]
    for j, ref in enumerate(pieces):
        at = pl.multiple_of((where_ref[0] ^ j) * fan, 16)
        kv_ref[pl.ds(at, fan), :] = ref[:, :two]
        q_ref[pl.ds(at, fan), :] = ref[:, two:]


def collect(at, pieces):
    fan, three = pieces[0].shape
    cols = three // 3
    shape = lambda n: jax.ShapeDtypeStruct((fan * len(pieces), n), jnp.bfloat16)
    return pl.pallas_call(
        collect_kernel,
        in_specs=[SMEM] + [VMEM] * len(pieces),
        out_specs=[VMEM, VMEM],
        out_shape=[shape(2 * cols), shape(cols)],
        name="collect",
    )(at, *pieces)


def weave_kernel(where_ref, *refs, plan, fan, group):
    pieces, out_ref = refs[:-1], refs[-1]
    cols = out_ref.shape[1] // group
    for ref, (j, first) in zip(pieces, plan):
        for p in range(ref.shape[0] // fan):
            w = ref[p * fan:(p + 1) * fan]
            parts = natural([w[:, b * cols:(b + 1) * cols] for b in range(group)], where_ref[0])
            to = pl.multiple_of(((first + p) * group + (where_ref[0] ^ j)) * fan, 16)
            for b in range(group):
                out_ref[pl.ds(to, fan), b * cols:(b + 1) * cols] = parts[b]


def weave(at, blocks, fan, group):
    plan, pieces = [], []
    for j, block in enumerate(blocks):
        first = 0
        for piece in block:
            plan.append((j, first))
            pieces.append(piece)
            first += piece.shape[0] // fan
    rows = sum(p.shape[0] for p in pieces)
    return pl.pallas_call(
        partial(weave_kernel, plan=plan, fan=fan, group=group),
        in_specs=[SMEM] + [VMEM] * len(pieces),
        out_specs=VMEM,
        out_shape=jax.ShapeDtypeStruct((rows, pieces[0].shape[1]), jnp.bfloat16),
        name="weave",
    )(at, *pieces)


def swap_matrix():
    i = lax.broadcasted_iota(jnp.int32, (CHUNK, CHUNK), 0)
    j = lax.broadcasted_iota(jnp.int32, (CHUNK, CHUNK), 1)
    return jnp.where(j == (i % RATE) * RATE + i // RATE, 1.0, 0.0).astype(jnp.bfloat16)


def attention_kernel(where_ref, *refs, group, width, layout, back, counts):
    n_q, n_kv, n_prev = counts
    q_refs, kv_refs, prev_refs = refs[:n_q], refs[n_q:n_q + n_kv], refs[n_q + n_kv:n_q + n_kv + n_prev]
    outs = refs[n_q + n_kv + n_prev:n_q + n_kv + n_prev + group]
    qs, ks, vs, b1, b4, b16, acc, top, den, done_at, lse_at = refs[n_q + n_kv + n_prev + group:]
    group_at, half_at, plane = where_ref[0], where_ref[1], where_ref[2]
    heads = width // HEAD_SIZE
    chunks = qs.shape[0]
    held = ks.shape[0] - chunks
    per_block = chunks // group
    swap = swap_matrix()
    lane = lax.broadcasted_iota(jnp.int32, (1, width), 1)

    def place(spot):
        j, half, sub, subs = spot
        inner = sub if half is None else (half_at ^ half) * subs + sub
        return (group_at ^ j) * per_block + inner

    def swapped(rows):
        return jnp.dot(swap, rows, preferred_element_type=jnp.float32)

    def rows_from(refs, pieces):
        got = [refs[i][first:first + size] for i, first, size in pieces]
        return got[0] if len(got) == 1 else jnp.concatenate(got, 0)

    for spot, pieces in layout:
        n = place(spot)
        qs[n] = (swapped(rows_from(q_refs, pieces)) * HEAD_SIZE ** -0.5).astype(jnp.bfloat16)
        x = swapped(rows_from(kv_refs, pieces))
        ks[held + n] = x[:, :width].astype(jnp.bfloat16)
        vs[held + n] = x[:, width:].astype(jnp.bfloat16)
    for step, spot, pieces in back:
        n = held - step * chunks + place(spot)
        x = swapped(rows_from(prev_refs, pieces))
        ks[n] = x[:, :width].astype(jnp.bfloat16)
        vs[n] = x[:, width:].astype(jnp.bfloat16)

    def bias(ref, position_q, position_k):
        rows, cols = ref.shape[0] // heads, ref.shape[1]
        q = position_q(lax.broadcasted_iota(jnp.int32, (rows, cols), 0))
        k = position_k(lax.broadcasted_iota(jnp.int32, (rows, cols), 1))
        dist = q - k
        off = jnp.where((dist >= 0) & (dist <= KEYS_BEHIND), 0.0, NEG)
        for h in range(heads):
            ref[h * rows:(h + 1) * rows] = off

    bias(b16, lambda i: i + held * RATE, lambda j: j)
    bias(b4, lambda i: 4 * ((i // 64) * RATE + i % RATE) + (i % 64) // RATE + KEYS_BEHIND,
         lambda j: 4 * ((j // 64) * RATE + j % RATE) + (j % 64) // RATE)
    bias(b1, lambda i: RATE * (i % RATE) + i // RATE + CHUNK,
         lambda j: (j // CHUNK) * CHUNK + RATE * (j % RATE) + (j % CHUNK) // RATE)

    def absent(n):
        if n >= held:
            return None
        return jnp.where(plane * chunks + n - held >= 0, 0.0, NEG)

    def per_head(x, rows):
        if heads == 1:
            return jnp.broadcast_to(x, (rows, width))
        out = x[(heads - 1) * rows:]
        for h in reversed(range(heads - 1)):
            out = jnp.where(lane < (h + 1) * HEAD_SIZE, x[h * rows:(h + 1) * rows], out)
        return jnp.broadcast_to(out, (rows, width))

    def block(q, k, v, off):
        rows = q.shape[0]
        if heads > 1:
            zero = jnp.zeros_like(q)
            q = jnp.concatenate([jnp.where(lane // HEAD_SIZE == h, q, zero) for h in range(heads)], 0)
        score = lax.dot_general(q, k, (((1,), (1,)), ((), ())), preferred_element_type=jnp.float32) + off
        high = jnp.max(score, axis=-1, keepdims=True)
        weight = jnp.exp(score - high)
        total = jnp.sum(weight, axis=-1, keepdims=True)
        out = jnp.dot(weight.astype(jnp.bfloat16), v, preferred_element_type=jnp.float32)
        return per_head(out, rows), per_head(high, rows), per_head(total, rows)

    def merged(old, new):
        (o0, m0, l0), (o1, m1, l1) = old, new
        m = jnp.maximum(m0, m1)
        e0, e1 = jnp.exp(m0 - m), jnp.exp(m1 - m)
        return o0 * e0 + o1 * e1, m, l0 * e0 + l1 * e1

    def masked(ref, rows_per_chunk, where_chunks):
        off = ref[...]
        gone = [absent(n) for n in where_chunks]
        if all(x is None for x in gone):
            return off
        col = lax.broadcasted_iota(jnp.int32, (1, off.shape[1]), 1) // rows_per_chunk
        add = jnp.zeros((1, off.shape[1]), jnp.float32)
        for at, x in enumerate(gone):
            if x is not None:
                add = jnp.where(col == at, x, add)
        return off + add

    def rows_of(ref, picks):
        return jnp.concatenate([ref[n, r * RATE:(r + 1) * RATE] for n, r in picks], 0)

    def put(picks, values):
        for at, (n, r) in enumerate(picks):
            for ref, x in zip((acc, top, den), values):
                ref[n, r * RATE:(r + 1) * RATE] = x[at * RATE:(at + 1) * RATE]

    off16 = masked(b16, RATE, range(held + chunks))
    for r in range(RATE):
        picks = [(n, r) for n in range(chunks)]
        keys = [(n, r) for n in range(held + chunks)]
        put(picks, block(rows_of(qs, picks), rows_of(ks, keys), rows_of(vs, keys), off16))

    for two in range(0, chunks, 2):
        off4 = masked(b4, 64, [held + two - 2, held + two - 1, held + two, held + two + 1])
        for c in range(4):
            picks = [(n, c + 4 * i) for n in (two, two + 1) for i in range(4)]
            keys = [(n, c + 4 * i) for n in range(held + two - 2, held + two + 2) for i in range(4)]
            new = block(rows_of(qs, picks), rows_of(ks, keys), rows_of(vs, keys), off4)
            put(picks, merged([rows_of(ref, picks) for ref in (acc, top, den)], new))

    part = CHUNK // 2
    for n in range(chunks):
        k = jnp.concatenate([ks[held + n - 1], ks[held + n]], 0)
        v = jnp.concatenate([vs[held + n - 1], vs[held + n]], 0)
        done, lses = [], []
        for p in range(2):
            rows = slice(p * part, (p + 1) * part)
            off = masked(b1, CHUNK, [held + n - 1, held + n])
            off = jnp.concatenate([off[h * CHUNK + p * part:h * CHUNK + (p + 1) * part] for h in range(heads)], 0)
            new = block(qs[n, rows], k, v, off)
            o, m, l = merged([ref[n, rows] for ref in (acc, top, den)], new)
            done.append((o / l).astype(jnp.bfloat16))
            lses.append(m + jnp.log(l))
        done_at[n] = swapped(jnp.concatenate(done, 0)).astype(jnp.bfloat16)
        lse = jnp.concatenate(lses, 0).T
        for h in range(heads):
            lse_at[n, h:h + 1] = lse[h * HEAD_SIZE:h * HEAD_SIZE + 1]

    for j, out in enumerate(outs):
        lines = []
        for c in range(per_block):
            n = (group_at ^ j) * per_block + c
            out[c * CHUNK:(c + 1) * CHUNK] = done_at[n]
            lse = lse_at[n]
            for h in range(heads):
                for at in range(0, CHUNK, width):
                    lines.append(lse[h:h + 1, at:at + width])
        size = -(-len(lines) // 16) * 16
        if size > len(lines):
            lines.append(jnp.zeros((size - len(lines), width), jnp.float32))
        rest = jnp.concatenate(lines, 0)
        for t in range(3):
            some = rest.astype(jnp.bfloat16)
            rest = rest - some.astype(jnp.float32)
            first = per_block * CHUNK + t * size
            out[first:first + size] = some


def lse_lines(rows, heads, width):
    used = rows * heads // width
    return used, -(-used // 16) * 16


def attention(at, qs, kvs, prevs, layout, back, group, rows):
    width = qs[0].shape[1]
    heads = width // HEAD_SIZE
    chunks = rows * group // CHUNK
    held = KEYS_BEHIND * RATE // CHUNK
    _, size = lse_lines(rows, heads, width)
    state = pltpu.VMEM((chunks, CHUNK, width), jnp.float32)
    own = pltpu.VMEM((chunks, CHUNK, width), jnp.bfloat16)
    both = pltpu.VMEM((held + chunks, CHUNK, width), jnp.bfloat16)
    return pl.pallas_call(
        partial(attention_kernel, group=group, width=width, layout=layout, back=back,
                counts=(len(qs), len(kvs), len(prevs))),
        in_specs=[SMEM] + [VMEM] * (len(qs) + len(kvs) + len(prevs)),
        out_specs=[VMEM] * group,
        out_shape=[jax.ShapeDtypeStruct((rows + 3 * size, width), jnp.bfloat16)] * group,
        scratch_shapes=[
            own, both, both,
            pltpu.VMEM((heads * CHUNK, 2 * CHUNK), jnp.float32),
            pltpu.VMEM((heads * 128, 256), jnp.float32),
            pltpu.VMEM((heads * chunks * RATE, (held + chunks) * RATE), jnp.float32),
            state, state, state, own,
            pltpu.VMEM((chunks, 8, CHUNK), jnp.float32),
        ],
        name="dilated",
    )(at, *qs, *kvs, *prevs)


def shards(tokens, w_query, w_key, w_value, w_out):
    rows, model = tokens.shape
    _, width = w_query.shape
    devices, cores = lax.axis_size("sp"), lax.axis_size("tp")
    group = 4
    while width % (group * HEAD_SIZE) or devices % group:
        group //= 2
    planes = devices // group
    here, core = lax.axis_index("sp"), lax.axis_index("tp")
    group_at, plane = here % group, here // group
    cols = width // group
    heads = cols // HEAD_SIZE
    split = cores == 2 and group > 1
    at = jnp.stack([group_at, core if split else 0 * core, plane]).astype(jnp.int32)

    def across(x, step):
        return lax.ppermute(x, "sp", [(j, j ^ step) for j in range(devices)])

    def beyond(x, step):
        pairs = [(p * group + g, (p + step) * group + g) for p in range(planes - step) for g in range(group)]
        return lax.ppermute(x, "sp", pairs)

    def swapped(x):
        return lax.ppermute(x, "tp", [(0, 1), (1, 0)])

    def along(x):
        if planes > 8:
            lines = [[p * group + g for p in range(planes)] for g in range(group)]
            return lax.all_gather(x, "sp", axis=0, axis_index_groups=lines)
        out = jnp.zeros((planes + 1,) + x.shape, x.dtype)
        out = lax.dynamic_update_index_in_dim(out, x, plane, 0)
        up = down = x
        for s in range(1, planes):
            up_pairs = [(p, p + 1) for p in range(s - 1, planes - 1)]
            down_pairs = [(p, p - 1) for p in range(1, planes - s + 1)]
            up = lax.ppermute(up, "sp", [(p * group + g, q * group + g) for p, q in up_pairs for g in range(group)])
            down = lax.ppermute(down, "sp", [(p * group + g, q * group + g) for p, q in down_pairs for g in range(group)])
            out = lax.dynamic_update_index_in_dim(out, up, jnp.where(plane >= s, plane - s, planes), 0)
            out = lax.dynamic_update_index_in_dim(out, down, jnp.where(plane + s < planes, plane + s, planes), 0)
        return out[:planes]

    def gathered(x):
        if group == 1:
            return [[x]]
        one = across(x, 1)
        if group == 2:
            return [[x], [one]]
        two = across(x, 2)
        half = x.shape[0] // 2
        return [[x], [one], [two], [across(two[:half], 1), across(one[half:], 2)]]

    pieces = prep(at, w_query, w_key, w_value, group)
    pieces = [pieces[0]] + [across(pieces[j], j) for j in range(1, group)]
    w_kv, w_q = collect(at, pieces)
    w_kv = along(w_kv).reshape(model, 2 * cols)
    w_q = along(w_q).reshape(model, cols)

    share = rows // cores
    mine = lax.dynamic_slice_in_dim(tokens, core * share, share, 0)
    held_rows = [[tokens]]
    for block in gathered(mine)[1:]:
        if split:
            held_rows.append(block + [swapped(x) for x in block])
        else:
            held_rows.append([lax.all_gather(jnp.concatenate(block, 0), "tp", axis=0, tiled=True)])

    layout, index = [], 0
    offsets = []
    for j, block in enumerate(held_rows):
        ends = []
        for i, piece in enumerate(block):
            ends += [(index + i, r) for r in range(0, piece.shape[0], 128)]
        for c in range(rows // CHUNK):
            marks = ends[2 * c:2 * c + 2]
            if marks[0][0] == marks[1][0]:
                got = [(marks[0][0], marks[0][1], CHUNK)]
            else:
                got = [(i, r, 128) for i, r in marks]
            subs = share // CHUNK
            spot = (j, c // subs, c % subs, subs) if split and j else (j, None, c, 0)
            layout.append((spot, got))
            offsets.append((j, c))
        index += len(block)

    flat = [x for block in held_rows for x in block]

    def project(x, w):
        return jnp.dot(x, w, preferred_element_type=jnp.float32).astype(jnp.bfloat16)

    kvs = [project(x, w_kv) for x in flat]
    qs = [project(x, w_q) for x in flat]

    early = sum(len(block) for block in held_rows[:max(group - 1, 1)])
    loads = [kvs[:early], kvs[early:]]
    loads = [jnp.concatenate(x, 0) if len(x) > 1 else x[0] for x in loads if x]
    reach = (KEYS_BEHIND * RATE + rows * group - 1) // (rows * group)
    prevs, back = [], []
    for s in range(reach, 0, -1):
        for (spot, _), (j, c) in zip(layout, offsets):
            late = j >= max(group - 1, 1)
            first = ((j - max(group - 1, 1)) if late else j) * rows + c * CHUNK
            back.append((s, spot, [(len(prevs) + int(late), first, CHUNK)]))
        prevs += [beyond(x, s) for x in loads]

    w_line = along(w_out.T).reshape(-1, width)
    w_rows = weave(at, gathered(w_line), w_out.shape[1], group)

    outs = attention(at, qs, kvs, prevs, layout, back, group, rows)
    outs = [outs[0]] + [across(outs[j], j) for j in range(1, group)]
    att = jnp.concatenate([x[:rows] for x in outs], 1)
    used, size = lse_lines(rows, heads, cols)

    def lse_of(x):
        x = sum(x[rows + t * size:rows + t * size + used].astype(jnp.float32) for t in range(3))
        x = x.reshape(rows // CHUNK, heads, RATE, RATE)
        return x.transpose(1, 0, 3, 2).reshape(heads, rows)

    row_lse = jnp.concatenate(natural([lse_of(x) for x in outs], group_at), 0)

    def partial_out(x):
        return lax.dot_general(x, w_rows, (((1,), (1,)), ((), ())), preferred_element_type=jnp.float32).astype(jnp.bfloat16)

    if cores == 2:
        other = partial_out(lax.dynamic_slice_in_dim(att, (1 - core) * share, share, 0))
        got = swapped(other)
        own = partial_out(lax.dynamic_slice_in_dim(att, core * share, share, 0))
        mixed = (own.astype(jnp.float32) + got.astype(jnp.float32)).astype(jnp.bfloat16)
    else:
        mixed = lax.psum_scatter(partial_out(att), "tp", scatter_dimension=0, tiled=True)
    return (mixed, row_lse)


def solution(mesh):
    placed = (P("sp", None), P("sp", "tp"), P("sp", "tp"), P("sp", "tp"), P("tp", "sp"))

    return jax.shard_map(
        shards,
        mesh=mesh,
        in_specs=placed,
        out_specs=(P(("sp", "tp"), None), P("tp", "sp")),
        check_vma=False,
    )
```

profile of v0, /device:TPU:0, one launch (start us, length us, event | category | flops | bytes accessed | tf_op | source)
XLA Modules:
  0.0 233.2 jit_solution(17563201910897664721)
XLA Ops:
  3.8 3.0 %collective-permute-start.9 = (bf16[256,3072]{1,0:T(8,128)(2,1)}, bf16[256,3072]{1,0:T(8,128)(2,1)}, u32[]{:S(2)}, u32[]{:S(2)}) collective-permute-start(bf16[256,3072]{1,0:T(8,128)(2,1)} %constant_dynamic-slice_fusion), channel_id=1, source_target_pairs={{0,2},{2,0},{4,6},{6,4},{8,10},{10,8},{12,14},{14,12},{16,18},{18,... | collective-permute-start | bytes 4718600 | tf_op jit(solution)/shard_map/ppermute | solution.py:313
  11.5 3.0 %collective-permute-start.2 = (bf16[192,384]{1,0:T(8,128)(2,1)}, bf16[192,384]{1,0:T(8,128)(2,1)}, u32[]{:S(2)}, u32[]{:S(2)}) collective-permute-start(bf16[192,384]{1,0:T(8,128)(2,1)} %get-tuple-element.15), channel_id=1, source_target_pairs={{0,6},{2,4},{4,2},{6,0},{8,14},{10,12},{12,10},{14,8},{16,22},{18,... | collective-permute-start | bytes 442376 | tf_op jit(solution)/shard_map/ppermute | solution.py:313
  16.1 29.2 %collective-permute-done.refs_1_ = bf16[192,384]{1,0:T(8,128)(2,1)S(1)} collective-permute-done((bf16[192,384]{1,0:T(8,128)(2,1)}, bf16[192,384]{1,0:T(8,128)(2,1)S(1)}, u32[]{:S(2)}, u32[]{:S(2)}) %collective-permute-start) | collective-permute-done | bytes 147488 | tf_op jit(solution)/shard_map/ppermute | solution.py:313
  45.4 4.7 %collective-permute-start.28 = (bf16[192,512]{1,0:T(8,128)(2,1)S(1)}, bf16[192,512]{1,0:T(8,128)(2,1)}, u32[]{:S(2)}, u32[]{:S(2)}) collective-permute-start(bf16[192,512]{1,0:T(8,128)(2,1)S(1)} %bitcast.125), channel_id=1, source_target_pairs={{0,8},{2,10},{4,12},{6,14},{8,16},{10,18},{12,20},{14,22},{16,24},... | collective-permute-start | bytes 589832 | tf_op jit(solution)/shard_map/ppermute | solution.py:332
  53.4 4.7 %collective-permute-start.17 = (bf16[768,256]{1,0:T(8,128)(2,1)}, bf16[768,256]{1,0:T(8,128)(2,1)S(1)}, u32[]{:S(2)}, u32[]{:S(2)}) collective-permute-start(bf16[768,256]{1,0:T(8,128)(2,1)} %get-tuple-element.17), channel_id=1, source_target_pairs={{0,8},{2,10},{4,12},{6,14},{8,16},{10,18},{12,20},{14,22},{16,24},... | collective-permute-start | bytes 1179656 | tf_op jit(solution)/shard_map/ppermute | solution.py:332
  61.4 4.5 %collective-permute-start.3 = (bf16[768,128]{1,0:T(8,128)(2,1)S(1)}, bf16[768,128]{1,0:T(8,128)(2,1)S(1)}, u32[]{:S(2)}, u32[]{:S(2)}) collective-permute-start(bf16[768,128]{1,0:T(8,128)(2,1)S(1)} %copy-done.12), channel_id=1, source_target_pairs={{0,8},{2,10},{4,12},{6,14},{8,16},{10,18},{12,20},{14,22},{16,24},... | collective-permute-start | bytes 589832 | tf_op jit(solution)/shard_map/ppermute | solution.py:332
  70.4 6.7 %collective-permute-done.4 = bf16[768,128]{1,0:T(8,128)(2,1)S(1)} collective-permute-done((bf16[768,128]{1,0:T(8,128)(2,1)S(1)}, bf16[768,128]{1,0:T(8,128)(2,1)S(1)}, u32[]{:S(2)}, u32[]{:S(2)}) %collective-permute-start.4) | collective-permute-done | bytes 196640 | tf_op jit(solution)/shard_map/ppermute | solution.py:333
  79.8 11.1 %collective-permute-done.31 = bf16[192,512]{1,0:T(8,128)(2,1)S(1)} collective-permute-done((bf16[192,512]{1,0:T(8,128)(2,1)S(1)}, bf16[192,512]{1,0:T(8,128)(2,1)S(1)}, u32[]{:S(2)}, u32[]{:S(2)}) %collective-permute-start.31) | collective-permute-done | bytes 196640 | tf_op jit(solution)/shard_map/ppermute | solution.py:333
  95.8 5.6 %collective-permute-done.6 = bf16[768,128]{1,0:T(8,128)(2,1)S(1)} collective-permute-done((bf16[768,128]{1,0:T(8,128)(2,1)S(1)}, bf16[768,128]{1,0:T(8,128)(2,1)S(1)}, u32[]{:S(2)}, u32[]{:S(2)}) %collective-permute-start.6) | collective-permute-done | bytes 196640 | tf_op jit(solution)/shard_map/ppermute | solution.py:333
  109.5 6.2 %collective-permute-done.8 = bf16[768,128]{1,0:T(8,128)(2,1)S(1)} collective-permute-done((bf16[768,128]{1,0:T(8,128)(2,1)S(1)}, bf16[768,128]{1,0:T(8,128)(2,1)S(1)}, u32[]{:S(2)}, u32[]{:S(2)}) %collective-permute-start.8) | collective-permute-done | bytes 196640 | tf_op jit(solution)/shard_map/ppermute | solution.py:333
  122.6 6.7 %collective-permute-done.22 = bf16[768,256]{1,0:T(8,128)(2,1)S(1)} collective-permute-done((bf16[768,256]{1,0:T(8,128)(2,1)S(1)}, bf16[768,256]{1,0:T(8,128)(2,1)S(1)}, u32[]{:S(2)}, u32[]{:S(2)}) %collective-permute-start.22) | collective-permute-done | bytes 393248 | tf_op jit(solution)/shard_map/ppermute | solution.py:333
  133.5 7.4 %collective-permute-done.34.refs_1_ = bf16[768,512]{1,0:T(8,128)(2,1)S(1)} collective-permute-done((bf16[768,512]{1,0:T(8,128)(2,1)S(1)}, bf16[768,512]{1,0:T(8,128)(2,1)S(1)}, u32[]{:S(2)}, u32[]{:S(2)}) %collective-permute-start.34) | collective-permute-done | bytes 786464 | tf_op jit(solution)/shard_map/ppermute | solution.py:313
  146.8 2.6 %convolution_convert_fusion.13.refs_3_ = bf16[256,128]{1,0:T(8,128)(2,1)} fusion(bf16[256,3072]{1,0:T(8,128)(2,1)} %collective-permute-done.11, bf16[3072,128]{1,0:T(8,128)(2,1)S(1)} %bitcast.105), kind=kOutput, calls=%fused_computation.18 | convolution fusion | flops 201359360 | bytes 2424832 | tf_op jit(solution)/shard_map/dot_general | solution.py:384
  149.4 2.6 %convolution_convert_fusion.15.refs_1_ = bf16[256,128]{1,0:T(8,128)(2,1)} fusion(bf16[256,3072]{1,0:T(8,128)(2,1)} %collective-permute-done.9, bf16[3072,128]{1,0:T(8,128)(2,1)S(1)} %bitcast.106), kind=kOutput, calls=%fused_computation.20 | convolution fusion | flops 201359360 | bytes 2424832 | tf_op jit(solution)/shard_map/dot_general | solution.py:384
  152.0 2.6 %constant_dynamic-update-slice_fusion.3 = (bf16[1536,256]{1,0:T(8,128)(2,1)S(1)}, bf16[256,256]{1,0:T(8,128)(2,1)}) fusion(bf16[1536,256]{1,0:T(8,128)(2,1)S(1)} %get-tuple-element.28, bf16[256,3072]{1,0:T(8,128)(2,1)} %collective-permute-done.9, bf16[3072,256]{1,0:T(8,128)(2,1)S(1)} %bitcast.114), kind=kOutput, calls=%fused_computation.54 | convolution fusion | flops 402718720 | bytes 3407872 | tf_op jit(solution)/shard_map/dot_general | solution.py:384
  155.4 4.2 %collective-permute-done.13 = bf16[128,3072]{1,0:T(8,128)(2,1)S(1)} collective-permute-done((bf16[128,3072]{1,0:T(8,128)(2,1)S(1)}, bf16[128,3072]{1,0:T(8,128)(2,1)S(1)}, u32[]{:S(2)}, u32[]{:S(2)}) %collective-permute-start.13) | collective-permute-done | bytes 786464 | tf_op jit(solution)/shard_map/ppermute | solution.py:313
  163.3 4.3 %collective-permute-start.24 = (bf16[512,256]{1,0:T(8,128)(2,1)S(1)}, bf16[512,256]{1,0:T(8,128)(2,1)S(1)}, u32[]{:S(2)}, u32[]{:S(2)}) collective-permute-start(bf16[512,256]{1,0:T(8,128)(2,1)S(1)} %pad_maximum_fusion.1), channel_id=1, source_target_pairs={{0,8},{2,10},{4,12},{6,14},{8,16},{10,18},{12,20},{14,22},{16,24},... | collective-permute-start | bytes 786440 | tf_op jit(solution)/shard_map/ppermute | solution.py:317
  168.9 2.6 %constant_dynamic-update-slice_fusion.1 = (bf16[1536,256]{1,0:T(8,128)(2,1)S(1)}, bf16[256,256]{1,0:T(8,128)(2,1)}) fusion(bf16[1536,256]{1,0:T(8,128)(2,1)S(1)} %get-tuple-element.32, bf16[256,3072]{1,0:T(8,128)(2,1)} %collective-permute-done.11, bf16[3072,256]{1,0:T(8,128)(2,1)S(1)} %bitcast.120), kind=kOutput, calls=%fused_computation.52 | convolution fusion | flops 402718720 | bytes 3407872 | tf_op jit(solution)/shard_map/dot_general | solution.py:384
  172.7 6.8 %collective-permute-start.23 = (bf16[1536,256]{1,0:T(8,128)(2,1)S(1)}, bf16[1536,256]{1,0:T(8,128)(2,1)}, u32[]{:S(2)}, u32[]{:S(2)}) collective-permute-start(bf16[1536,256]{1,0:T(8,128)(2,1)S(1)} %get-tuple-element.36), channel_id=1, source_target_pairs={{0,8},{2,10},{4,12},{6,14},{8,16},{10,18},{12,20},{14,22},{16,24},... | collective-permute-start | bytes 2359304 | tf_op jit(solution)/shard_map/ppermute | solution.py:317
  184.5 10.9 %collective-permute-done.23.refs_18_ = bf16[1536,256]{1,0:T(8,128)(2,1)} collective-permute-done((bf16[1536,256]{1,0:T(8,128)(2,1)S(1)}, bf16[1536,256]{1,0:T(8,128)(2,1)}, u32[]{:S(2)}, u32[]{:S(2)}) %collective-permute-start.23) | collective-permute-done | bytes 786464 | tf_op jit(solution)/shard_map/ppermute | solution.py:317
  195.5 13.2 %dilated.1 = (bf16[560,128]{1,0:T(8,128)(2,1)}, bf16[560,128]{1,0:T(8,128)(2,1)}, bf16[560,128]{1,0:T(8,128)(2,1)}, bf16[560,128]{1,0:T(8,128)(2,1)}) custom-call(s32[3]{0:T(128)} %pad_add_fusion.where_ref, bf16[512,128]{1,0:T(8,128)(2,1)} %fusion.4.refs_0_, bf16[256,128]{1,0:T(8,128)(2,1)} %convolution_convert_fusion.15.refs_1_, ...), custom_call_target="tpu_custom_call" | custom-call | tf_op jit(solution)/shard_map/dilated/pallas_call | solution.py:279
  212.2 4.6 %weave.1 = bf16[3072,512]{1,0:T(8,128)(2,1)} custom-call(s32[3]{0:T(128)} %pad_add_fusion.where_ref, bf16[768,512]{1,0:T(8,128)(2,1)} %bitcast.124, bf16[768,512]{1,0:T(8,128)(2,1)} %copy-done.4, bf16[768,512]{1,0:T(8,128)(2,1)} %copy-done.3, bf16[384,512]{1,0:T(8,128)(2,1)} %collective-permute-done.36.refs_3_, bf16[384,512]{1,0:T(8,128)(2,1)} %collective-permute-done.37.refs_4_), custom_call_target="tpu_custom_call" | custom-call | tf_op jit(solution)/shard_map/weave/pallas_call | solution.py:95
  220.6 4.3 %convolution_convert_fusion = bf16[256,3072]{1,0:T(8,128)(2,1)} fusion(bf16[3072,512]{1,0:T(8,128)(2,1)} %weave.1, bf16[512,512]{1,0:T(8,128)(2,1)S(1)} %pad_maximum_fusion, s32[]{:T(128)S(6)} %select_n.189), kind=kOutput, calls=%fused_computation | convolution fusion | flops 806092800 | bytes 4980740 | tf_op jit(solution)/shard_map/dot_general | solution.py:417
  228.6 4.6 %fusion.2 = bf16[256,3072]{1,0:T(8,128)(2,1)} fusion(bf16[3072,512]{1,0:T(8,128)(2,1)} %weave.1, bf16[256,3072]{1,0:T(8,128)(2,1)} %collective-permute-done.38, bf16[512,512]{1,0:T(8,128)(2,1)} %copy-done.2, s32[]{:T(128)S(6)} %select_n.188), kind=kOutput, calls=%fused_computation.4 | convolution fusion | flops 809238528 | bytes 6553604 | tf_op jit(solution)/shard_map/dot_general | solution.py:417
  (163 shorter events, 75.9 us)
Async XLA Ops:
  3.8 138.0 %collective-permute-start.9 = (bf16[256,3072]{1,0:T(8,128)(2,1)}, bf16[256,3072]{1,0:T(8,128)(2,1)}, u32[]{:S(2)}, u32[]{:S(2)}) collective-permute-start(bf16[256,3072]{1,0:T(8,128)(2,1)} %constant_dynamic-slice_fusion), channel_id=1, source_target_pairs={{0,2},{2,0},{4,6},{6,4},{8,10},{10,8},{12,14},{14,12},{16,18},{18,... | collective-permute-start | bytes 4718600 | tf_op jit(solution)/shard_map/ppermute | solution.py:313
  6.7 136.8 %collective-permute-start.11 = (bf16[256,3072]{1,0:T(8,128)(2,1)}, bf16[256,3072]{1,0:T(8,128)(2,1)}, u32[]{:S(2)}, u32[]{:S(2)}) collective-permute-start(bf16[256,3072]{1,0:T(8,128)(2,1)} %constant_dynamic-slice_fusion), channel_id=1, source_target_pairs={{0,4},{2,6},{4,0},{6,2},{8,12},{10,14},{12,8},{14,10},{16,20},{18,... | collective-permute-start | bytes 4718600 | tf_op jit(solution)/shard_map/ppermute | solution.py:313
  10.9 34.4 %collective-permute-start = (bf16[192,384]{1,0:T(8,128)(2,1)}, bf16[192,384]{1,0:T(8,128)(2,1)S(1)}, u32[]{:S(2)}, u32[]{:S(2)}) collective-permute-start(bf16[192,384]{1,0:T(8,128)(2,1)} %get-tuple-element.13), channel_id=1, source_target_pairs={{0,2},{2,0},{4,6},{6,4},{8,10},{10,8},{12,14},{14,12},{16,18},{18,... | collective-permute-start | bytes 442376 | tf_op jit(solution)/shard_map/ppermute | solution.py:313
  11.5 38.6 %collective-permute-start.1 = (bf16[192,384]{1,0:T(8,128)(2,1)}, bf16[192,384]{1,0:T(8,128)(2,1)}, u32[]{:S(2)}, u32[]{:S(2)}) collective-permute-start(bf16[192,384]{1,0:T(8,128)(2,1)} %get-tuple-element.14), channel_id=1, source_target_pairs={{0,4},{2,6},{4,0},{6,2},{8,12},{10,14},{12,8},{14,10},{16,20},{18,... | collective-permute-start | bytes 442376 | tf_op jit(solution)/shard_map/ppermute | solution.py:313
  11.5 39.9 %collective-permute-start.2 = (bf16[192,384]{1,0:T(8,128)(2,1)}, bf16[192,384]{1,0:T(8,128)(2,1)}, u32[]{:S(2)}, u32[]{:S(2)}) collective-permute-start(bf16[192,384]{1,0:T(8,128)(2,1)} %get-tuple-element.15), channel_id=1, source_target_pairs={{0,6},{2,4},{4,2},{6,0},{8,14},{10,12},{12,10},{14,8},{16,22},{18,... | collective-permute-start | bytes 442376 | tf_op jit(solution)/shard_map/ppermute | solution.py:313
  45.4 13.1 %collective-permute-start.28 = (bf16[192,512]{1,0:T(8,128)(2,1)S(1)}, bf16[192,512]{1,0:T(8,128)(2,1)}, u32[]{:S(2)}, u32[]{:S(2)}) collective-permute-start(bf16[192,512]{1,0:T(8,128)(2,1)S(1)} %bitcast.125), channel_id=1, source_target_pairs={{0,8},{2,10},{4,12},{6,14},{8,16},{10,18},{12,20},{14,22},{16,24},... | collective-permute-start | bytes 589832 | tf_op jit(solution)/shard_map/ppermute | solution.py:332
  50.0 11.4 %collective-permute-start.29 = (bf16[192,512]{1,0:T(8,128)(2,1)S(1)}, bf16[192,512]{1,0:T(8,128)(2,1)S(1)}, u32[]{:S(2)}, u32[]{:S(2)}) collective-permute-start(bf16[192,512]{1,0:T(8,128)(2,1)S(1)} %bitcast.126), channel_id=1, source_target_pairs={{8,0},{10,2},{12,4},{14,6},{16,8},{18,10},{20,12},{22,14},{24,16},... | collective-permute-start | bytes 589832 | tf_op jit(solution)/shard_map/ppermute | solution.py:333
  53.4 39.0 %collective-permute-start.17 = (bf16[768,256]{1,0:T(8,128)(2,1)}, bf16[768,256]{1,0:T(8,128)(2,1)S(1)}, u32[]{:S(2)}, u32[]{:S(2)}) collective-permute-start(bf16[768,256]{1,0:T(8,128)(2,1)} %get-tuple-element.17), channel_id=1, source_target_pairs={{0,8},{2,10},{4,12},{6,14},{8,16},{10,18},{12,20},{14,22},{16,24},... | collective-permute-start | bytes 1179656 | tf_op jit(solution)/shard_map/ppermute | solution.py:332
  58.5 35.2 %collective-permute-start.18 = (bf16[768,256]{1,0:T(8,128)(2,1)S(1)}, bf16[768,256]{1,0:T(8,128)(2,1)S(1)}, u32[]{:S(2)}, u32[]{:S(2)}) collective-permute-start(bf16[768,256]{1,0:T(8,128)(2,1)S(1)} %copy-done.9), channel_id=1, source_target_pairs={{8,0},{10,2},{12,4},{14,6},{16,8},{18,10},{20,12},{22,14},{24,16},... | collective-permute-start | bytes 1179656 | tf_op jit(solution)/shard_map/ppermute | solution.py:333
  77.8 13.1 %collective-permute-start.31 = (bf16[192,512]{1,0:T(8,128)(2,1)S(1)}, bf16[192,512]{1,0:T(8,128)(2,1)S(1)}, u32[]{:S(2)}, u32[]{:S(2)}) collective-permute-start(bf16[192,512]{1,0:T(8,128)(2,1)S(1)} %collective-permute-done.29), channel_id=1, source_target_pairs={{8,0},{10,2},{12,4},{14,6},{16,8},{18,10},{20,12},{22,14},{9,1},{1... | collective-permute-start | bytes 589832 | tf_op jit(solution)/shard_map/ppermute | solution.py:333
  94.4 11.1 %collective-permute-start.33 = (bf16[192,512]{1,0:T(8,128)(2,1)S(1)}, bf16[192,512]{1,0:T(8,128)(2,1)S(1)}, u32[]{:S(2)}, u32[]{:S(2)}) collective-permute-start(bf16[192,512]{1,0:T(8,128)(2,1)S(1)} %collective-permute-done.31), channel_id=1, source_target_pairs={{8,0},{10,2},{12,4},{14,6},{9,1},{11,3},{13,5},{15,7}} | collective-permute-start | bytes 589832 | tf_op jit(solution)/shard_map/ppermute | solution.py:333
  101.3 17.6 %collective-permute-start.19 = (bf16[768,256]{1,0:T(8,128)(2,1)S(1)}, bf16[768,256]{1,0:T(8,128)(2,1)S(1)}, u32[]{:S(2)}, u32[]{:S(2)}) collective-permute-start(bf16[768,256]{1,0:T(8,128)(2,1)S(1)} %collective-permute-done.17), channel_id=1, source_target_pairs={{8,16},{10,18},{12,20},{14,22},{16,24},{18,26},{20,28},{22,30},{9,... | collective-permute-start | bytes 1179656 | tf_op jit(solution)/shard_map/ppermute | solution.py:332
  102.1 17.6 %collective-permute-start.20 = (bf16[768,256]{1,0:T(8,128)(2,1)S(1)}, bf16[768,256]{1,0:T(8,128)(2,1)S(1)}, u32[]{:S(2)}, u32[]{:S(2)}) collective-permute-start(bf16[768,256]{1,0:T(8,128)(2,1)S(1)} %collective-permute-done.18), channel_id=1, source_target_pairs={{8,0},{10,2},{12,4},{14,6},{16,8},{18,10},{20,12},{22,14},{9,1},{1... | collective-permute-start | bytes 1179656 | tf_op jit(solution)/shard_map/ppermute | solution.py:333
  115.7 15.5 %collective-permute-start.35 = (bf16[768,512]{1,0:T(8,128)(2,1)S(1)}, bf16[768,512]{1,0:T(8,128)(2,1)S(1)}, u32[]{:S(2)}, u32[]{:S(2)}) collective-permute-start(bf16[768,512]{1,0:T(8,128)(2,1)S(1)} %bitcast.122), channel_id=1, source_target_pairs={{0,4},{2,6},{4,0},{6,2},{8,12},{10,14},{12,8},{14,10},{16,20},{18,... | collective-permute-start | bytes 2359304 | tf_op jit(solution)/shard_map/ppermute | solution.py:313
  119.6 9.7 %collective-permute-start.22 = (bf16[768,256]{1,0:T(8,128)(2,1)S(1)}, bf16[768,256]{1,0:T(8,128)(2,1)S(1)}, u32[]{:S(2)}, u32[]{:S(2)}) collective-permute-start(bf16[768,256]{1,0:T(8,128)(2,1)S(1)} %collective-permute-done.20), channel_id=1, source_target_pairs={{8,0},{10,2},{12,4},{14,6},{9,1},{11,3},{13,5},{15,7}} | collective-permute-start | bytes 1179656 | tf_op jit(solution)/shard_map/ppermute | solution.py:333
  121.0 19.9 %collective-permute-start.34 = (bf16[768,512]{1,0:T(8,128)(2,1)S(1)}, bf16[768,512]{1,0:T(8,128)(2,1)S(1)}, u32[]{:S(2)}, u32[]{:S(2)}) collective-permute-start(bf16[768,512]{1,0:T(8,128)(2,1)S(1)} %bitcast.123), channel_id=1, source_target_pairs={{0,2},{2,0},{4,6},{6,4},{8,10},{10,8},{12,14},{14,12},{16,18},{18,... | collective-permute-start | bytes 2359304 | tf_op jit(solution)/shard_map/ppermute | solution.py:313
  132.0 80.2 %collective-permute-start.36 = (bf16[384,512]{1,0:T(8,128)(2,1)}, bf16[384,512]{1,0:T(8,128)(2,1)}, u32[]{:S(2)}, u32[]{:S(2)}) collective-permute-start(bf16[384,512]{1,0:T(8,128)(2,1)} %slice.100), channel_id=1, source_target_pairs={{0,2},{2,0},{4,6},{6,4},{8,10},{10,8},{12,14},{14,12},{16,18},{18,... | collective-permute-start | bytes 1179656 | tf_op jit(solution)/shard_map/ppermute | solution.py:313
  142.9 12.1 %collective-permute-start.14 = (bf16[128,3072]{1,0:T(8,128)(2,1)S(1)}, bf16[128,3072]{1,0:T(8,128)(2,1)S(1)}, u32[]{:S(2)}, u32[]{:S(2)}) collective-permute-start(bf16[128,3072]{1,0:T(8,128)(2,1)S(1)} %slice.94), channel_id=1, source_target_pairs={{0,4},{2,6},{4,0},{6,2},{8,12},{10,14},{12,8},{14,10},{16,20},{18,... | collective-permute-start | bytes 2359304 | tf_op jit(solution)/shard_map/ppermute | solution.py:313
  144.7 14.9 %collective-permute-start.13 = (bf16[128,3072]{1,0:T(8,128)(2,1)S(1)}, bf16[128,3072]{1,0:T(8,128)(2,1)S(1)}, u32[]{:S(2)}, u32[]{:S(2)}) collective-permute-start(bf16[128,3072]{1,0:T(8,128)(2,1)S(1)} %slice.93), channel_id=1, source_target_pairs={{0,2},{2,0},{4,6},{6,4},{8,10},{10,8},{12,14},{14,12},{16,18},{18,... | collective-permute-start | bytes 2359304 | tf_op jit(solution)/shard_map/ppermute | solution.py:313
  146.3 21.3 %collective-permute-start.10 = (bf16[256,3072]{1,0:T(8,128)(2,1)}, bf16[256,3072]{1,0:T(8,128)(2,1)S(1)}, u32[]{:S(2)}, u32[]{:S(2)}) collective-permute-start(bf16[256,3072]{1,0:T(8,128)(2,1)} %collective-permute-done.9), channel_id=1, source_target_pairs={{0,1},{1,0},{2,3},{3,2},{4,5},{5,4},{6,7},{7,6},{8,9},{9,8},{10,11... | collective-permute-start | bytes 4718600 | tf_op jit(solution)/shard_map/ppermute | solution.py:320
  146.3 25.2 %collective-permute-start.12 = (bf16[256,3072]{1,0:T(8,128)(2,1)}, bf16[256,3072]{1,0:T(8,128)(2,1)S(1)}, u32[]{:S(2)}, u32[]{:S(2)}) collective-permute-start(bf16[256,3072]{1,0:T(8,128)(2,1)} %collective-permute-done.11), channel_id=1, source_target_pairs={{0,1},{1,0},{2,3},{3,2},{4,5},{5,4},{6,7},{7,6},{8,9},{9,8},{10,11... | collective-permute-start | bytes 4718600 | tf_op jit(solution)/shard_map/ppermute | solution.py:320
  162.0 50.2 %collective-permute-start.37 = (bf16[384,512]{1,0:T(8,128)(2,1)}, bf16[384,512]{1,0:T(8,128)(2,1)}, u32[]{:S(2)}, u32[]{:S(2)}) collective-permute-start(bf16[384,512]{1,0:T(8,128)(2,1)} %slice.101), channel_id=1, source_target_pairs={{0,4},{2,6},{4,0},{6,2},{8,12},{10,14},{12,8},{14,10},{16,20},{18,... | collective-permute-start | bytes 1179656 | tf_op jit(solution)/shard_map/ppermute | solution.py:313
  163.3 20.5 %collective-permute-start.24 = (bf16[512,256]{1,0:T(8,128)(2,1)S(1)}, bf16[512,256]{1,0:T(8,128)(2,1)S(1)}, u32[]{:S(2)}, u32[]{:S(2)}) collective-permute-start(bf16[512,256]{1,0:T(8,128)(2,1)S(1)} %pad_maximum_fusion.1), channel_id=1, source_target_pairs={{0,8},{2,10},{4,12},{6,14},{8,16},{10,18},{12,20},{14,22},{16,24},... | collective-permute-start | bytes 786440 | tf_op jit(solution)/shard_map/ppermute | solution.py:317
  172.7 22.7 %collective-permute-start.23 = (bf16[1536,256]{1,0:T(8,128)(2,1)S(1)}, bf16[1536,256]{1,0:T(8,128)(2,1)}, u32[]{:S(2)}, u32[]{:S(2)}) collective-permute-start(bf16[1536,256]{1,0:T(8,128)(2,1)S(1)} %get-tuple-element.36), channel_id=1, source_target_pairs={{0,8},{2,10},{4,12},{6,14},{8,16},{10,18},{12,20},{14,22},{16,24},... | collective-permute-start | bytes 2359304 | tf_op jit(solution)/shard_map/ppermute | solution.py:317
  (30 other events, 176.9 us)
where the time goes:
time: 235 us; the launch traced here: 233 us
  waiting for transfers between devices  95 us (40%)
  starting transfers between devices  59.8 us (25%)
  matrix products  33 us (14%)
  Pallas kernels  21.8 us (9%)
  local copies, waits for them, and re-layouts  19.6 us (8%)
  other arithmetic  2.73 us (1%)
    ppermute x14, waiting for transfers between devices, across(): return lax.ppermute(x, 'sp', [(j, j ^ step) for j in range(devices)])  43.1 us
    ppermute x9, waiting for transfers between devices, along(): lax.ppermute(down, 'sp', [(p * group + g, q * group + g) for p, q in down...  37.8 us
    dot_general x18, matrix products, project(): jnp.dot(x, w, preferred_element_type=jnp.float32).astype(jnp.bfloat16)  24.1 us
    ppermute x14, starting transfers between devices, across(): return lax.ppermute(x, 'sp', [(j, j ^ step) for j in range(devices)])  18.7 us
    ppermute x9, starting transfers between devices, along(): lax.ppermute(up, 'sp', [(p * group + g, q * group + g) for p, q in up_pai...  17.9 us
    pallas_call x1, Pallas kernels, attention(): pl.pallas_call(partial(attention_kernel, group=group, width=width, layout...  13.2 us
    ppermute x9, starting transfers between devices, along(): lax.ppermute(down, 'sp', [(p * group + g, q * group + g) for p, q in down...  11.6 us
    ppermute x2, starting transfers between devices, beyond(): return lax.ppermute(x, 'sp', pairs)  11.1 us
  transfers between devices with their start and end apart: 39, of which 14 were waited for; matrix products, arithmetic and copies ran while one was open for 18% of the time, Pallas kernels for 9%

commit v1 on v0

--- a/solution.py
+++ b/solution.py
@@ -69,6 +69,30 @@
         out_shape=[shape(2 * cols), shape(cols)],
         name="collect",
     )(at, *pieces)
+
+
+def line_kernel(where_ref, *refs):
+    ins, out_ref = refs[:-1], refs[-1]
+    plane, planes = where_ref[2], out_ref.shape[0]
+    out_ref[plane] = ins[0][...]
+    for s in range(1, planes):
+        @pl.when(plane >= s)
+        def _():
+            out_ref[jnp.maximum(plane - s, 0)] = ins[2 * s - 1][...]
+
+        @pl.when(plane + s < planes)
+        def _():
+            out_ref[jnp.minimum(plane + s, planes - 1)] = ins[2 * s][...]
+
+
+def line(at, parts, planes):
+    return pl.pallas_call(
+        line_kernel,
+        in_specs=[SMEM] + [VMEM] * len(parts),
+        out_specs=VMEM,
+        out_shape=jax.ShapeDtypeStruct((planes,) + parts[0].shape, jnp.bfloat16),
+        name="line",
+    )(at, *parts)
 
 
 def weave_kernel(where_ref, *refs, plan, fan, group):
@@ -319,23 +343,33 @@
     def swapped(x):
         return lax.ppermute(x, "tp", [(0, 1), (1, 0)])
 
-    def along(x):
+    def along(x, eager):
         if planes > 8:
             lines = [[p * group + g for p in range(planes)] for g in range(group)]
             return lax.all_gather(x, "sp", axis=0, axis_index_groups=lines)
-        out = jnp.zeros((planes + 1,) + x.shape, x.dtype)
-        out = lax.dynamic_update_index_in_dim(out, x, plane, 0)
+        out = None
+        if eager:
+            out = jnp.zeros((planes + 1,) + x.shape, x.dtype)
+            out = lax.dynamic_update_index_in_dim(out, x, plane, 0)
+        parts = [x]
         up = down = x
         for s in range(1, planes):
             up_pairs = [(p, p + 1) for p in range(s - 1, planes - 1)]
             down_pairs = [(p, p - 1) for p in range(1, planes - s + 1)]
             up = lax.ppermute(up, "sp", [(p * group + g, q * group + g) for p, q in up_pairs for g in range(group)])
             down = lax.ppermute(down, "sp", [(p * group + g, q * group + g) for p, q in down_pairs for g in range(group)])
-            out = lax.dynamic_update_index_in_dim(out, up, jnp.where(plane >= s, plane - s, planes), 0)
-            out = lax.dynamic_update_index_in_dim(out, down, jnp.where(plane + s < planes, plane + s, planes), 0)
-        return out[:planes]
-
-    def gathered(x):
+            parts += [up, down]
+            if eager:
+                out = lax.dynamic_update_index_in_dim(out, up, jnp.where(plane >= s, plane - s, planes), 0)
+                out = lax.dynamic_update_index_in_dim(out, down, jnp.where(plane + s < planes, plane + s, planes), 0)
+        return out[:planes] if eager else parts
+
+    def lined(parts, late):
+        if planes > 8:
+            return parts
+        return line(lax.optimization_barrier((at, late))[0], parts, planes)
+
+    def gathered(x, cut=None):
         if group == 1:
             return [[x]]
         one = across(x, 1)
@@ -343,18 +377,24 @@
             return [[x], [one]]
         two = across(x, 2)
         half = x.shape[0] // 2
-        return [[x], [one], [two], [across(two[:half], 1), across(one[half:], 2)]]
+        first, second = two[:half], one[half:]
+        if cut is not None:
+            cut += [first, second]
+        return [[x], [one], [two], [across(first, 1), across(second, 2)]]
 
     pieces = prep(at, w_query, w_key, w_value, group)
     pieces = [pieces[0]] + [across(pieces[j], j) for j in range(1, group)]
     w_kv, w_q = collect(at, pieces)
-    w_kv = along(w_kv).reshape(model, 2 * cols)
-    w_q = along(w_q).reshape(model, cols)
+    w_kv = along(w_kv, True).reshape(model, 2 * cols)
+    q_parts = along(w_q, False)
 
     share = rows // cores
     mine = lax.dynamic_slice_in_dim(tokens, core * share, share, 0)
     held_rows = [[tokens]]
-    for block in gathered(mine)[1:]:
+    passed = []
+    gotten = gathered(mine, passed)
+    w_kv = lax.optimization_barrier((w_kv, *passed))[0]
+    for block in gotten[1:]:
         if split:
             held_rows.append(block + [swapped(x) for x in block])
         else:
@@ -383,12 +423,16 @@
     def project(x, w):
         return jnp.dot(x, w, preferred_element_type=jnp.float32).astype(jnp.bfloat16)
 
-    kvs = [project(x, w_kv) for x in flat]
+    early = sum(len(block) for block in held_rows[:max(group - 1, 1)])
+    kvs = [project(x, w_kv) for x in flat[:early]]
+    loads = [jnp.concatenate(kvs, 0)]
+    if early < len(flat):
+        flat[early:] = lax.optimization_barrier((*flat[early:], loads[0]))[:-1]
+        kvs += [project(x, w_kv) for x in flat[early:]]
+        loads.append(jnp.concatenate(kvs[early:], 0))
+    w_q = lined(q_parts, loads[0]).reshape(model, cols)
     qs = [project(x, w_q) for x in flat]
 
-    early = sum(len(block) for block in held_rows[:max(group - 1, 1)])
-    loads = [kvs[:early], kvs[early:]]
-    loads = [jnp.concatenate(x, 0) if len(x) > 1 else x[0] for x in loads if x]
     reach = (KEYS_BEHIND * RATE + rows * group - 1) // (rows * group)
     prevs, back = [], []
     for s in range(reach, 0, -1):
@@ -398,7 +442,7 @@
             back.append((s, spot, [(len(prevs) + int(late), first, CHUNK)]))
         prevs += [beyond(x, s) for x in loads]
 
-    w_line = along(w_out.T).reshape(-1, width)
+    w_line = lined(along(w_out.T, False), loads[0]).reshape(-1, width)
     w_rows = weave(at, gathered(w_line), w_out.shape[1], group)
 
     outs = attention(at, qs, kvs, prevs, layout, back, group, rows)

time: 235 us -> 226 us (0.962)
  waiting for transfers between devices: 95 us -> 72.9 us
  matrix products: 33 us -> 44.5 us
  Pallas kernels: 21.8 us -> 26.7 us
  starting transfers between devices: 59.8 us -> 56.2 us
    dot_general x18, matrix products: 24.1 us -> 35.8 us  [project(): jnp.dot(x, w, preferred_element_type=jnp.float32).astype(jnp.bfloat16)]
    ppermute x2, waiting for transfers between devices: 10.9 us -> 0.01 us  [beyond(): return lax.ppermute(x, 'sp', pairs)]
    ppermute x14, waiting for transfers between devices: 43.1 us -> 37 us  [across(): return lax.ppermute(x, 'sp', [(j, j ^ step) for j in range(devices)])]
    pallas_call x0 -> x2, Pallas kernels: none -> 4.93 us  [line(): pl.pallas_call(line_kernel, in_specs=[SMEM] + [VMEM] * len(parts), out_sp...]
    ppermute x9, waiting for transfers between devices: 37.8 us -> 33.9 us  [along(): lax.ppermute(down, 'sp', [(p * group + g, q * group + g) for p, q in down...]
    ppermute x2, starting transfers between devices: 11.1 us -> 7.77 us  [beyond(): return lax.ppermute(x, 'sp', pairs)]
    unnamed x30 -> x48, local copies, waits for them, and re-layouts: 2.64 us -> 5.7 us
    slice x7 -> x5, local copies, waits for them, and re-layouts: 5.36 us -> 6.02 us  [the longest x4 5.92 us: gathered(): first, second = (two[:half], one[half:])]
  transfers between devices with their start and end apart: 39 -> 39, of which waited for: 14 -> 15; matrix products, arithmetic and copies ran while one was open for 18% -> 23% of each run, Pallas kernels for 9% -> 10%
where the time goes in v1:
time: 226 us; the launch traced here: 225 us
  waiting for transfers between devices  72.9 us (32%)
  starting transfers between devices  56.2 us (25%)
  matrix products  44.5 us (20%)
  Pallas kernels  26.7 us (12%)
  local copies, waits for them, and re-layouts  18.9 us (8%)
  other arithmetic  4.27 us (2%)
    ppermute x14, waiting for transfers between devices, across(): return lax.ppermute(x, 'sp', [(j, j ^ step) for j in range(devices)])  37 us
    dot_general x18, matrix products, project(): jnp.dot(x, w, preferred_element_type=jnp.float32).astype(jnp.bfloat16)  35.8 us
    ppermute x9, waiting for transfers between devices, along(): lax.ppermute(down, 'sp', [(p * group + g, q * group + g) for p, q in down...  33.9 us
    ppermute x14, starting transfers between devices, across(): return lax.ppermute(x, 'sp', [(j, j ^ step) for j in range(devices)])  19.3 us
    ppermute x9, starting transfers between devices, along(): lax.ppermute(up, 'sp', [(p * group + g, q * group + g) for p, q in up_pai...  16.3 us
    pallas_call x1, Pallas kernels, attention(): pl.pallas_call(partial(attention_kernel, group=group, width=width, layout...  13.3 us
    ppermute x9, starting transfers between devices, along(): lax.ppermute(down, 'sp', [(p * group + g, q * group + g) for p, q in down...  11.5 us
    dot_general x2, matrix products, partial_out(): lax.dot_general(x, w_rows, (((1,), (1,)), ((), ())), preferred_element_ty...  8.74 us
  transfers between devices with their start and end apart: 39, of which 15 were waited for; matrix products, arithmetic and copies ran while one was open for 23% of the time, Pallas kernels for 10%

profile of v1, /device:TPU:0, one launch (start us, length us, event | category | flops | bytes accessed | tf_op | source)
XLA Modules:
  0.0 224.6 jit_solution(14115906990220528945)
XLA Ops:
  3.8 3.0 %collective-permute-start.10 = (bf16[256,3072]{1,0:T(8,128)(2,1)}, bf16[256,3072]{1,0:T(8,128)(2,1)}, u32[]{:S(2)}, u32[]{:S(2)}) collective-permute-start(bf16[256,3072]{1,0:T(8,128)(2,1)} %constant_dynamic-slice_fusion), channel_id=1, source_target_pairs={{0,2},{2,0},{4,6},{6,4},{8,10},{10,8},{12,14},{14,12},{16,18},{18,... | collective-permute-start | bytes 4718600 | tf_op jit(solution)/shard_map/ppermute | solution.py:337
  11.5 3.0 %collective-permute-start.2 = (bf16[192,384]{1,0:T(8,128)(2,1)}, bf16[192,384]{1,0:T(8,128)(2,1)}, u32[]{:S(2)}, u32[]{:S(2)}) collective-permute-start(bf16[192,384]{1,0:T(8,128)(2,1)} %get-tuple-element.21), channel_id=1, source_target_pairs={{0,6},{2,4},{4,2},{6,0},{8,14},{10,12},{12,10},{14,8},{16,22},{18,... | collective-permute-start | bytes 442376 | tf_op jit(solution)/shard_map/ppermute | solution.py:337
  14.4 30.9 %collective-permute-done.refs_1_ = bf16[192,384]{1,0:T(8,128)(2,1)S(1)} collective-permute-done((bf16[192,384]{1,0:T(8,128)(2,1)}, bf16[192,384]{1,0:T(8,128)(2,1)S(1)}, u32[]{:S(2)}, u32[]{:S(2)}) %collective-permute-start) | collective-permute-done | bytes 147488 | tf_op jit(solution)/shard_map/ppermute | solution.py:337
  45.4 3.8 %collective-permute-done.1.refs_2_ = bf16[192,384]{1,0:T(8,128)(2,1)S(1)} collective-permute-done((bf16[192,384]{1,0:T(8,128)(2,1)}, bf16[192,384]{1,0:T(8,128)(2,1)S(1)}, u32[]{:S(2)}, u32[]{:S(2)}) %collective-permute-start.1) | collective-permute-done | bytes 147488 | tf_op jit(solution)/shard_map/ppermute | solution.py:337
  51.8 4.2 %collective-permute-start.3 = (bf16[768,256]{1,0:T(8,128)(2,1)}, bf16[768,256]{1,0:T(8,128)(2,1)}, u32[]{:S(2)}, u32[]{:S(2)}) collective-permute-start(bf16[768,256]{1,0:T(8,128)(2,1)} %get-tuple-element.22), channel_id=1, source_target_pairs={{0,8},{2,10},{4,12},{6,14},{8,16},{10,18},{12,20},{14,22},{16,24},... | collective-permute-start | bytes 1179656 | tf_op jit(solution)/shard_map/ppermute | solution.py:359
  57.4 5.3 %collective-permute-start.28 = (bf16[192,512]{1,0:T(8,128)(2,1)}, bf16[192,512]{1,0:T(8,128)(2,1)}, u32[]{:S(2)}, u32[]{:S(2)}) collective-permute-start(bf16[192,512]{1,0:T(8,128)(2,1)} %bitcast.96), channel_id=1, source_target_pairs={{0,8},{2,10},{4,12},{6,14},{8,16},{10,18},{12,20},{14,22},{16,24},... | collective-permute-start | bytes 589832 | tf_op jit(solution)/shard_map/ppermute | solution.py:359
  70.1 9.0 %collective-permute-done.6 = bf16[768,256]{1,0:T(8,128)(2,1)S(1)} collective-permute-done((bf16[768,256]{1,0:T(8,128)(2,1)S(1)}, bf16[768,256]{1,0:T(8,128)(2,1)S(1)}, u32[]{:S(2)}, u32[]{:S(2)}) %collective-permute-start.6) | collective-permute-done | bytes 393248 | tf_op jit(solution)/shard_map/ppermute | solution.py:360
  84.0 4.8 %collective-permute-done.8 = bf16[768,256]{1,0:T(8,128)(2,1)S(1)} collective-permute-done((bf16[768,256]{1,0:T(8,128)(2,1)S(1)}, bf16[768,256]{1,0:T(8,128)(2,1)S(1)}, u32[]{:S(2)}, u32[]{:S(2)}) %collective-permute-start.8) | collective-permute-done | bytes 393248 | tf_op jit(solution)/shard_map/ppermute | solution.py:360
  88.8 3.3 %collective-permute-start.20 = (bf16[128,3072]{1,0:T(8,128)(2,1)S(1)}, bf16[128,3072]{1,0:T(8,128)(2,1)}, u32[]{:S(2)}, u32[]{:S(2)}) collective-permute-start(bf16[128,3072]{1,0:T(8,128)(2,1)S(1)} %slice.86), channel_id=1, source_target_pairs={{0,4},{2,6},{4,0},{6,2},{8,12},{10,14},{12,8},{14,10},{16,20},{18,... | collective-permute-start | bytes 2359304 | tf_op jit(solution)/shard_map/ppermute | solution.py:337
  96.1 4.5 %collective-permute-done.29.refs_2_ = bf16[192,512]{1,0:T(8,128)(2,1)S(1)} collective-permute-done((bf16[192,512]{1,0:T(8,128)(2,1)S(1)}, bf16[192,512]{1,0:T(8,128)(2,1)S(1)}, u32[]{:S(2)}, u32[]{:S(2)}) %collective-permute-start.29) | collective-permute-done | bytes 196640 | tf_op jit(solution)/shard_map/ppermute | solution.py:360
  102.0 2.7 %constant_dynamic-update-slice_fusion.3 = (bf16[1536,256]{1,0:T(8,128)(2,1)}, bf16[256,256]{1,0:T(8,128)(2,1)}) fusion(bf16[1536,256]{1,0:T(8,128)(2,1)} %get-tuple-element.40, bf16[256,3072]{1,0:T(8,128)(2,1)} %collective-permute-done.10, bf16[3072,256]{1,0:T(8,128)(2,1)S(1)} %bitcast.85), kind=kOutput, calls=%fused_computation.40 | convolution fusion | flops 402718720 | bytes 3407872 | tf_op jit(solution)/shard_map/dot_general | solution.py:424
  109.0 4.1 %collective-permute-done.14.refs_2_ = bf16[768,128]{1,0:T(8,128)(2,1)S(1)} collective-permute-done((bf16[768,128]{1,0:T(8,128)(2,1)S(1)}, bf16[768,128]{1,0:T(8,128)(2,1)S(1)}, u32[]{:S(2)}, u32[]{:S(2)}) %collective-permute-start.14) | collective-permute-done | bytes 196640 | tf_op jit(solution)/shard_map/ppermute | solution.py:360
  115.9 2.7 %constant_dynamic-update-slice_fusion.1 = (bf16[1536,256]{1,0:T(8,128)(2,1)}, bf16[256,256]{1,0:T(8,128)(2,1)}) fusion(bf16[1536,256]{1,0:T(8,128)(2,1)} %get-tuple-element.44, bf16[256,3072]{1,0:T(8,128)(2,1)} %collective-permute-done.9, bf16[3072,256]{1,0:T(8,128)(2,1)S(1)} %bitcast.87), kind=kOutput, calls=%fused_computation.38 | convolution fusion | flops 402718720 | bytes 3407872 | tf_op jit(solution)/shard_map/dot_general | solution.py:424
  118.5 3.9 %collective-permute-done.31.refs_4_ = bf16[192,512]{1,0:T(8,128)(2,1)S(1)} collective-permute-done((bf16[192,512]{1,0:T(8,128)(2,1)S(1)}, bf16[192,512]{1,0:T(8,128)(2,1)S(1)}, u32[]{:S(2)}, u32[]{:S(2)}) %collective-permute-start.31) | collective-permute-done | bytes 196640 | tf_op jit(solution)/shard_map/ppermute | solution.py:360
  127.1 5.3 %collective-permute-done.16.refs_4_ = bf16[768,128]{1,0:T(8,128)(2,1)} collective-permute-done((bf16[768,128]{1,0:T(8,128)(2,1)S(1)}, bf16[768,128]{1,0:T(8,128)(2,1)}, u32[]{:S(2)}, u32[]{:S(2)}) %collective-permute-start.16) | collective-permute-done | bytes 196640 | tf_op jit(solution)/shard_map/ppermute | solution.py:360
  136.1 5.8 %collective-permute-start.23 = (bf16[1536,256]{1,0:T(8,128)(2,1)}, bf16[1536,256]{1,0:T(8,128)(2,1)}, u32[]{:S(2)}, u32[]{:S(2)}) collective-permute-start(bf16[1536,256]{1,0:T(8,128)(2,1)} %get-tuple-element.48), channel_id=1, source_target_pairs={{0,8},{2,10},{4,12},{6,14},{8,16},{10,18},{12,20},{14,22},{16,24},... | collective-permute-start | bytes 2359304 | tf_op jit(solution)/shard_map/ppermute | solution.py:341
  154.8 2.6 %line.2 = bf16[4,768,128]{2,1,0:T(8,128)(2,1)} custom-call(s32[3]{0:T(128)} %pad_add_fusion.where_ref, bf16[768,128]{1,0:T(8,128)(2,1)} %get-tuple-element.25.refs_0_, bf16[768,128]{1,0:T(8,128)(2,1)} %copy-done.15, bf16[768,128]{1,0:T(8,128)(2,1)} %copy-done.16, bf16[768,128]{1,0:T(8,128)(2,1)} %collective-permute-done.15.refs_3_, ...), custom_call_target="tpu_custom_call" | custom-call | tf_op jit(solution)/shard_map/line/pallas_call | solution.py:89
  159.8 2.6 %convolution_convert_fusion.12.refs_4_ = bf16[256,128]{1,0:T(8,128)(2,1)} fusion(bf16[256,3072]{1,0:T(8,128)(2,1)} %copy-done.6, bf16[3072,128]{1,0:T(8,128)(2,1)S(1)} %bitcast.76), kind=kOutput, calls=%fused_computation.17 | convolution fusion | flops 201359360 | bytes 2424832 | tf_op jit(solution)/shard_map/dot_general | solution.py:424
  162.4 2.7 %convolution_convert_fusion.13.refs_3_ = bf16[256,128]{1,0:T(8,128)(2,1)} fusion(bf16[256,3072]{1,0:T(8,128)(2,1)} %collective-permute-done.9, bf16[3072,128]{1,0:T(8,128)(2,1)S(1)} %bitcast.77), kind=kOutput, calls=%fused_computation.18 | convolution fusion | flops 201359360 | bytes 2424832 | tf_op jit(solution)/shard_map/dot_general | solution.py:424
  166.3 2.6 %convolution_convert_fusion.15.refs_1_ = bf16[256,128]{1,0:T(8,128)(2,1)} fusion(bf16[256,3072]{1,0:T(8,128)(2,1)} %collective-permute-done.10, bf16[3072,128]{1,0:T(8,128)(2,1)S(1)} %bitcast.79), kind=kOutput, calls=%fused_computation.20 | convolution fusion | flops 201359360 | bytes 2424832 | tf_op jit(solution)/shard_map/dot_general | solution.py:424
  183.4 13.3 %dilated.1 = (bf16[560,128]{1,0:T(8,128)(2,1)}, bf16[560,128]{1,0:T(8,128)(2,1)}, bf16[560,128]{1,0:T(8,128)(2,1)}, bf16[560,128]{1,0:T(8,128)(2,1)}) custom-call(s32[3]{0:T(128)} %pad_add_fusion.where_ref, bf16[512,128]{1,0:T(8,128)(2,1)} %fusion.4.refs_0_, bf16[256,128]{1,0:T(8,128)(2,1)} %convolution_convert_fusion.15.refs_1_, ...), custom_call_target="tpu_custom_call" | custom-call | tf_op jit(solution)/shard_map/dilated/pallas_call | solution.py:303
  207.8 4.3 %weave.1 = bf16[3072,512]{1,0:T(8,128)(2,1)} custom-call(s32[3]{0:T(128)} %pad_add_fusion.where_ref, bf16[768,512]{1,0:T(8,128)(2,1)} %bitcast.95, bf16[768,512]{1,0:T(8,128)(2,1)} %collective-permute-done.34.refs_1_, bf16[768,512]{1,0:T(8,128)(2,1)} %collective-permute-done.35.refs_2_, bf16[384,512]{1,0:T(8,128)(2,1)} %copy-done.11, ...), custom_call_target="tpu_custom_call" | custom-call | tf_op jit(solution)/shard_map/weave/pallas_call | solution.py:119
  212.2 4.1 %convolution_convert_fusion = bf16[256,3072]{1,0:T(8,128)(2,1)} fusion(bf16[3072,512]{1,0:T(8,128)(2,1)} %weave.1, bf16[512,512]{1,0:T(8,128)(2,1)} %pad_maximum_fusion, s32[]{:T(128)S(6)} %select_n.161), kind=kOutput, calls=%fused_computation | convolution fusion | flops 806092800 | bytes 4980740 | tf_op jit(solution)/shard_map/dot_general | solution.py:461
  220.1 4.6 %fusion.2 = bf16[256,3072]{1,0:T(8,128)(2,1)} fusion(bf16[3072,512]{1,0:T(8,128)(2,1)} %weave.1, bf16[256,3072]{1,0:T(8,128)(2,1)} %collective-permute-done.38, bf16[512,512]{1,0:T(8,128)(2,1)} %pad_maximum_fusion, s32[]{:T(128)S(6)} %select_n.160), kind=kOutput, calls=%fused_computation.4 | convolution fusion | flops 809238528 | bytes 6553604 | tf_op jit(solution)/shard_map/dot_general | solution.py:461
  (165 shorter events, 90.4 us)
Async XLA Ops:
  3.8 76.6 %collective-permute-start.10 = (bf16[256,3072]{1,0:T(8,128)(2,1)}, bf16[256,3072]{1,0:T(8,128)(2,1)}, u32[]{:S(2)}, u32[]{:S(2)}) collective-permute-start(bf16[256,3072]{1,0:T(8,128)(2,1)} %constant_dynamic-slice_fusion), channel_id=1, source_target_pairs={{0,2},{2,0},{4,6},{6,4},{8,10},{10,8},{12,14},{14,12},{16,18},{18,... | collective-permute-start | bytes 4718600 | tf_op jit(solution)/shard_map/ppermute | solution.py:337
  6.7 73.8 %collective-permute-start.9 = (bf16[256,3072]{1,0:T(8,128)(2,1)}, bf16[256,3072]{1,0:T(8,128)(2,1)}, u32[]{:S(2)}, u32[]{:S(2)}) collective-permute-start(bf16[256,3072]{1,0:T(8,128)(2,1)} %constant_dynamic-slice_fusion), channel_id=1, source_target_pairs={{0,4},{2,6},{4,0},{6,2},{8,12},{10,14},{12,8},{14,10},{16,20},{18,... | collective-permute-start | bytes 4718600 | tf_op jit(solution)/shard_map/ppermute | solution.py:337
  10.9 34.4 %collective-permute-start = (bf16[192,384]{1,0:T(8,128)(2,1)}, bf16[192,384]{1,0:T(8,128)(2,1)S(1)}, u32[]{:S(2)}, u32[]{:S(2)}) collective-permute-start(bf16[192,384]{1,0:T(8,128)(2,1)} %get-tuple-element.19), channel_id=1, source_target_pairs={{0,2},{2,0},{4,6},{6,4},{8,10},{10,8},{12,14},{14,12},{16,18},{18,... | collective-permute-start | bytes 442376 | tf_op jit(solution)/shard_map/ppermute | solution.py:337
  11.5 37.7 %collective-permute-start.1 = (bf16[192,384]{1,0:T(8,128)(2,1)}, bf16[192,384]{1,0:T(8,128)(2,1)S(1)}, u32[]{:S(2)}, u32[]{:S(2)}) collective-permute-start(bf16[192,384]{1,0:T(8,128)(2,1)} %get-tuple-element.20), channel_id=1, source_target_pairs={{0,4},{2,6},{4,0},{6,2},{8,12},{10,14},{12,8},{14,10},{16,20},{18,... | collective-permute-start | bytes 442376 | tf_op jit(solution)/shard_map/ppermute | solution.py:337
  11.5 37.7 %collective-permute-start.2 = (bf16[192,384]{1,0:T(8,128)(2,1)}, bf16[192,384]{1,0:T(8,128)(2,1)}, u32[]{:S(2)}, u32[]{:S(2)}) collective-permute-start(bf16[192,384]{1,0:T(8,128)(2,1)} %get-tuple-element.21), channel_id=1, source_target_pairs={{0,6},{2,4},{4,2},{6,0},{8,14},{10,12},{12,10},{14,8},{16,22},{18,... | collective-permute-start | bytes 442376 | tf_op jit(solution)/shard_map/ppermute | solution.py:337
  51.8 12.6 %collective-permute-start.3 = (bf16[768,256]{1,0:T(8,128)(2,1)}, bf16[768,256]{1,0:T(8,128)(2,1)}, u32[]{:S(2)}, u32[]{:S(2)}) collective-permute-start(bf16[768,256]{1,0:T(8,128)(2,1)} %get-tuple-element.22), channel_id=1, source_target_pairs={{0,8},{2,10},{4,12},{6,14},{8,16},{10,18},{12,20},{14,22},{16,24},... | collective-permute-start | bytes 1179656 | tf_op jit(solution)/shard_map/ppermute | solution.py:359
  56.1 11.0 %collective-permute-start.4 = (bf16[768,256]{1,0:T(8,128)(2,1)}, bf16[768,256]{1,0:T(8,128)(2,1)S(1)}, u32[]{:S(2)}, u32[]{:S(2)}) collective-permute-start(bf16[768,256]{1,0:T(8,128)(2,1)} %get-tuple-element.22), channel_id=1, source_target_pairs={{8,0},{10,2},{12,4},{14,6},{16,8},{18,10},{20,12},{22,14},{24,16},... | collective-permute-start | bytes 1179656 | tf_op jit(solution)/shard_map/ppermute | solution.py:360
  57.4 34.9 %collective-permute-start.28 = (bf16[192,512]{1,0:T(8,128)(2,1)}, bf16[192,512]{1,0:T(8,128)(2,1)}, u32[]{:S(2)}, u32[]{:S(2)}) collective-permute-start(bf16[192,512]{1,0:T(8,128)(2,1)} %bitcast.96), channel_id=1, source_target_pairs={{0,8},{2,10},{4,12},{6,14},{8,16},{10,18},{12,20},{14,22},{16,24},... | collective-permute-start | bytes 589832 | tf_op jit(solution)/shard_map/ppermute | solution.py:359
  67.1 12.0 %collective-permute-start.6 = (bf16[768,256]{1,0:T(8,128)(2,1)S(1)}, bf16[768,256]{1,0:T(8,128)(2,1)S(1)}, u32[]{:S(2)}, u32[]{:S(2)}) collective-permute-start(bf16[768,256]{1,0:T(8,128)(2,1)S(1)} %collective-permute-done.4), channel_id=1, source_target_pairs={{8,0},{10,2},{12,4},{14,6},{16,8},{18,10},{20,12},{22,14},{9,1},{1... | collective-permute-start | bytes 1179656 | tf_op jit(solution)/shard_map/ppermute | solution.py:360
  69.4 11.7 %collective-permute-start.7 = (bf16[768,256]{1,0:T(8,128)(2,1)S(1)}, bf16[768,256]{1,0:T(8,128)(2,1)S(1)}, u32[]{:S(2)}, u32[]{:S(2)}) collective-permute-start(bf16[768,256]{1,0:T(8,128)(2,1)S(1)} %collective-permute-done.5), channel_id=1, source_target_pairs={{16,24},{18,26},{20,28},{22,30},{17,25},{19,27},{21,29},{23,31}} | collective-permute-start | bytes 1179656 | tf_op jit(solution)/shard_map/ppermute | solution.py:359
  80.4 26.8 %collective-permute-start.11 = (bf16[256,3072]{1,0:T(8,128)(2,1)}, bf16[256,3072]{1,0:T(8,128)(2,1)S(1)}, u32[]{:S(2)}, u32[]{:S(2)}) collective-permute-start(bf16[256,3072]{1,0:T(8,128)(2,1)} %collective-permute-done.10), channel_id=1, source_target_pairs={{0,1},{1,0},{2,3},{3,2},{4,5},{5,4},{6,7},{7,6},{8,9},{9,8},{10,11... | collective-permute-start | bytes 4718600 | tf_op jit(solution)/shard_map/ppermute | solution.py:344
  80.6 43.9 %collective-permute-start.12 = (bf16[256,3072]{1,0:T(8,128)(2,1)}, bf16[256,3072]{1,0:T(8,128)(2,1)S(1)}, u32[]{:S(2)}, u32[]{:S(2)}) collective-permute-start(bf16[256,3072]{1,0:T(8,128)(2,1)} %collective-permute-done.9), channel_id=1, source_target_pairs={{0,1},{1,0},{2,3},{3,2},{4,5},{5,4},{6,7},{7,6},{8,9},{9,8},{10,11... | collective-permute-start | bytes 4718600 | tf_op jit(solution)/shard_map/ppermute | solution.py:344
  82.3 24.1 %collective-permute-start.19 = (bf16[128,3072]{1,0:T(8,128)(2,1)S(1)}, bf16[128,3072]{1,0:T(8,128)(2,1)}, u32[]{:S(2)}, u32[]{:S(2)}) collective-permute-start(bf16[128,3072]{1,0:T(8,128)(2,1)S(1)} %slice.85), channel_id=1, source_target_pairs={{0,2},{2,0},{4,6},{6,4},{8,10},{10,8},{12,14},{14,12},{16,18},{18,... | collective-permute-start | bytes 2359304 | tf_op jit(solution)/shard_map/ppermute | solution.py:337
  88.8 18.4 %collective-permute-start.20 = (bf16[128,3072]{1,0:T(8,128)(2,1)S(1)}, bf16[128,3072]{1,0:T(8,128)(2,1)}, u32[]{:S(2)}, u32[]{:S(2)}) collective-permute-start(bf16[128,3072]{1,0:T(8,128)(2,1)S(1)} %slice.86), channel_id=1, source_target_pairs={{0,4},{2,6},{4,0},{6,2},{8,12},{10,14},{12,8},{14,10},{16,20},{18,... | collective-permute-start | bytes 2359304 | tf_op jit(solution)/shard_map/ppermute | solution.py:337
  107.2 37.1 %collective-permute-start.21 = (bf16[128,3072]{1,0:T(8,128)(2,1)}, bf16[128,3072]{1,0:T(8,128)(2,1)}, u32[]{:S(2)}, u32[]{:S(2)}) collective-permute-start(bf16[128,3072]{1,0:T(8,128)(2,1)} %collective-permute-done.19), channel_id=1, source_target_pairs={{0,1},{1,0},{2,3},{3,2},{4,5},{5,4},{6,7},{7,6},{8,9},{9,8},{10,11... | collective-permute-start | bytes 2359304 | tf_op jit(solution)/shard_map/ppermute | solution.py:344
  107.3 37.2 %collective-permute-start.22 = (bf16[128,3072]{1,0:T(8,128)(2,1)}, bf16[128,3072]{1,0:T(8,128)(2,1)}, u32[]{:S(2)}, u32[]{:S(2)}) collective-permute-start(bf16[128,3072]{1,0:T(8,128)(2,1)} %collective-permute-done.20), channel_id=1, source_target_pairs={{0,1},{1,0},{2,3},{3,2},{4,5},{5,4},{6,7},{7,6},{8,9},{9,8},{10,11... | collective-permute-start | bytes 2359304 | tf_op jit(solution)/shard_map/ppermute | solution.py:344
  132.5 20.4 %collective-permute-start.17 = (bf16[768,128]{1,0:T(8,128)(2,1)}, bf16[768,128]{1,0:T(8,128)(2,1)}, u32[]{:S(2)}, u32[]{:S(2)}) collective-permute-start(bf16[768,128]{1,0:T(8,128)(2,1)} %collective-permute-done.15.refs_3_), channel_id=1, source_target_pairs={{16,24},{18,26},{20,28},{22,30},{17,25},{19,27},{21,29},{23,31}} | collective-permute-start | bytes 589832 | tf_op jit(solution)/shard_map/ppermute | solution.py:359
  133.8 21.0 %collective-permute-start.18 = (bf16[768,128]{1,0:T(8,128)(2,1)}, bf16[768,128]{1,0:T(8,128)(2,1)}, u32[]{:S(2)}, u32[]{:S(2)}) collective-permute-start(bf16[768,128]{1,0:T(8,128)(2,1)} %collective-permute-done.16.refs_4_), channel_id=1, source_target_pairs={{8,0},{10,2},{12,4},{14,6},{9,1},{11,3},{13,5},{15,7}} | collective-permute-start | bytes 589832 | tf_op jit(solution)/shard_map/ppermute | solution.py:360
  136.1 47.3 %collective-permute-start.23 = (bf16[1536,256]{1,0:T(8,128)(2,1)}, bf16[1536,256]{1,0:T(8,128)(2,1)}, u32[]{:S(2)}, u32[]{:S(2)}) collective-permute-start(bf16[1536,256]{1,0:T(8,128)(2,1)} %get-tuple-element.48), channel_id=1, source_target_pairs={{0,8},{2,10},{4,12},{6,14},{8,16},{10,18},{12,20},{14,22},{16,24},... | collective-permute-start | bytes 2359304 | tf_op jit(solution)/shard_map/ppermute | solution.py:341
  144.3 30.4 %collective-permute-start.35 = (bf16[768,512]{1,0:T(8,128)(2,1)}, bf16[768,512]{1,0:T(8,128)(2,1)}, u32[]{:S(2)}, u32[]{:S(2)}) collective-permute-start(bf16[768,512]{1,0:T(8,128)(2,1)} %bitcast.93), channel_id=1, source_target_pairs={{0,4},{2,6},{4,0},{6,2},{8,12},{10,14},{12,8},{14,10},{16,20},{18,... | collective-permute-start | bytes 2359304 | tf_op jit(solution)/shard_map/ppermute | solution.py:337
  144.5 33.1 %collective-permute-start.34 = (bf16[768,512]{1,0:T(8,128)(2,1)}, bf16[768,512]{1,0:T(8,128)(2,1)}, u32[]{:S(2)}, u32[]{:S(2)}) collective-permute-start(bf16[768,512]{1,0:T(8,128)(2,1)} %bitcast.94), channel_id=1, source_target_pairs={{0,2},{2,0},{4,6},{6,4},{8,10},{10,8},{12,14},{14,12},{16,18},{18,... | collective-permute-start | bytes 2359304 | tf_op jit(solution)/shard_map/ppermute | solution.py:337
  152.8 30.6 %collective-permute-start.24 = (bf16[512,256]{1,0:T(8,128)(2,1)}, bf16[512,256]{1,0:T(8,128)(2,1)}, u32[]{:S(2)}, u32[]{:S(2)}) collective-permute-start(bf16[512,256]{1,0:T(8,128)(2,1)} %pad_maximum_fusion.1), channel_id=1, source_target_pairs={{0,8},{2,10},{4,12},{6,14},{8,16},{10,18},{12,20},{14,22},{16,24},... | collective-permute-start | bytes 786440 | tf_op jit(solution)/shard_map/ppermute | solution.py:341
  176.4 30.7 %collective-permute-start.36 = (bf16[384,512]{1,0:T(8,128)(2,1)}, bf16[384,512]{1,0:T(8,128)(2,1)S(1)}, u32[]{:S(2)}, u32[]{:S(2)}) collective-permute-start(bf16[384,512]{1,0:T(8,128)(2,1)} %slice.90), channel_id=1, source_target_pairs={{0,2},{2,0},{4,6},{6,4},{8,10},{10,8},{12,14},{14,12},{16,18},{18,... | collective-permute-start | bytes 1179656 | tf_op jit(solution)/shard_map/ppermute | solution.py:337
  179.4 27.7 %collective-permute-start.37 = (bf16[384,512]{1,0:T(8,128)(2,1)}, bf16[384,512]{1,0:T(8,128)(2,1)}, u32[]{:S(2)}, u32[]{:S(2)}) collective-permute-start(bf16[384,512]{1,0:T(8,128)(2,1)} %slice.91), channel_id=1, source_target_pairs={{0,4},{2,6},{4,0},{6,2},{8,12},{10,14},{12,8},{14,10},{16,20},{18,... | collective-permute-start | bytes 1179656 | tf_op jit(solution)/shard_map/ppermute | solution.py:337
  (39 other events, 256.0 us)
